TPU v7x, 32 devices: a whole 2x2x4 slice. The times are simulated.
32 devices in a mesh: grp: 2 (over y), st: 4 (over z), tp: 4 (over x, core).
Axes of the slice: x: 2, y: 2, z: 4, core: 2. Of those that a mesh axis runs over, the one named last changes fastest.
Arguments:
- tokens: bfloat16 [8192, 2048], P(('grp', 'st'), 'tp'), parts along dimension 0, may hold values from -6 to 6
- norm_gain: float32 [2048], replicated, may hold values from 0.1 to 1.9
- pool_weight: bfloat16 [4, 512, 512], P('tp'), may hold values from -0.25 to 0.25
- pool_scale: float32 [2048], P('tp'), may hold values from 0.1 to 1.9
- query_weight: bfloat16 [2048, 1024], P(None, 'tp'), may hold values from -3 to 3
- gate_weight: bfloat16 [2048, 8], replicated, may hold values from -0.125 to 0.125
- key_weight: bfloat16 [2048, 1024], P(None, 'tp'), may hold values from -0.125 to 0.125
- value_weight: bfloat16 [2048, 1024], P(None, 'tp'), may hold values from -0.125 to 0.125
- out_weight: bfloat16 [1024, 2048], P(None, 'tp'), may hold values from -0.1875 to 0.1875
- passage_gain: float32 [2048], replicated, may hold values from 0.1 to 1.9
- passage_store: bfloat16 [192, 64, 2048], P(('grp', 'st')), parts along dimension 0, may hold values from -6 to 6
- passage_ids: int32 [64, 4], P(('grp', 'st')), parts along dimension 0, may hold values from 0 to 95, as said below
Outputs:
- mixed: bfloat16 [8192, 2048], P(('grp', 'st'), 'tp'), parts along dimension 0
There are 2 independent parts, one for each index of `grp`. A program takes and returns all parts, laid end to end along the dimension named above; an argument that names none is the same for every part. Nothing has to cross between parts.
Inputs may be any that keep to these rules, and one draw needn't show every extreme that they name: `passage_ids`: the ids of the blocks of one index of st name at most 8 passages held by any one index of st, and exactly 8 held by some index.
All inputs are finite; a program needn't handle non-finite values.
Results may differ from a plain program's by a relative error of at most 0.009.
Values may be sent and summed in bfloat16 or wider, within the bound.
A program may use at most 128 MiB of HBM per device.

v0:
```python
import jax
import jax.numpy as jnp
from jax import lax
from jax.sharding import PartitionSpec as P

HD = 128
GROUPS = 4
SEQ_LEN = 256
BLK = 128
NPB = 4
PLEN = 64
P_DEV = 24
epsilon = 1e-06


def normalize_rows(fetched, passage_gain):
    wide_rows = fetched.astype(jnp.float32)
    inverse = lax.rsqrt(jnp.mean(wide_rows * wide_rows, axis=-1, keepdims=True) + epsilon)
    return (wide_rows * inverse * passage_gain).astype(jnp.bfloat16)


def project_rows(fetched, passage_gain, both_weights):
    count_rows = fetched.shape[0]
    flat_rows = normalize_rows(fetched.reshape(count_rows * PLEN, fetched.shape[2]), passage_gain)
    projected = jnp.dot(flat_rows, both_weights, preferred_element_type=jnp.float32).astype(
        jnp.bfloat16
    )
    return projected.reshape(count_rows, PLEN, both_weights.shape[1])


def per_device(
    tokens,
    norm_gain,
    pool_weight,
    pool_scale,
    query_weight,
    gate_weight,
    key_weight,
    value_weight,
    out_weight,
    passage_gain,
    passage_store,
    passage_ids,
):
    head_index = lax.axis_index("tp")
    tok_rows, width_local = tokens.shape
    full_width = width_local * lax.axis_size("tp")
    local_heads = query_weight.shape[1] // HD
    head_width = local_heads * HD
    wide_tokens = tokens.astype(jnp.float32)
    square_sums = lax.psum(jnp.sum(wide_tokens * wide_tokens, axis=1), "tp")
    inverse = lax.rsqrt(square_sums / full_width + epsilon)
    gain_local = lax.dynamic_slice_in_dim(norm_gain, head_index * width_local, width_local)
    normed = (wide_tokens * inverse[:, None] * gain_local[None, :]).astype(jnp.bfloat16)
    sequences = tok_rows // SEQ_LEN
    widest = 2**GROUPS
    window = jnp.left_shift(jnp.int32(2), head_index)
    grouped = normed.astype(jnp.float32).reshape(sequences, SEQ_LEN, width_local)
    running = jnp.cumsum(grouped, axis=1)
    padded = jnp.concatenate(
        [jnp.zeros((sequences, widest, width_local), jnp.float32), running], axis=1
    )
    lagged = lax.dynamic_slice_in_dim(padded, widest - window, SEQ_LEN, axis=1)
    position = jnp.arange(SEQ_LEN, dtype=jnp.int32)
    divisor = jnp.minimum(position + 1, window).astype(jnp.float32)
    pooled = (
        ((running - lagged) / divisor[None, :, None] - grouped)
        .astype(jnp.bfloat16)
        .reshape(tok_rows, width_local)
    )
    mixing = (
        jnp.dot(pooled, pool_weight[0], preferred_element_type=jnp.float32) * pool_scale[None, :]
    )
    gate_columns = lax.dynamic_slice_in_dim(
        gate_weight, head_index * local_heads, local_heads, axis=1
    )
    columns = lax.all_gather(normed, "tp", axis=1, tiled=True)
    query_sum = jnp.dot(columns, query_weight, preferred_element_type=jnp.float32)
    gate_sum = jnp.dot(columns, gate_columns, preferred_element_type=jnp.float32)
    queries = query_sum.astype(jnp.bfloat16)
    gating = jax.nn.sigmoid(gate_sum)
    flat_ids = passage_ids.reshape(-1)
    asked_count = flat_ids.shape[0]
    st_count = lax.axis_size("st")
    capacity = max(2, (asked_count + st_count - 1) // st_count)
    owners = flat_ids // P_DEV
    local_index = flat_ids % P_DEV
    order_index = jnp.arange(asked_count, dtype=jnp.int32)
    earlier = (owners[None, :] == owners[:, None]) & (order_index[None, :] < order_index[:, None])
    slot_index = jnp.sum(earlier.astype(jnp.int32), axis=1)
    position_flat = owners * capacity + slot_index
    slot_range = jnp.arange(st_count * capacity, dtype=jnp.int32)
    request_table = jnp.sum(
        jnp.where(position_flat[None, :] == slot_range[:, None], local_index[None, :], 0), axis=1
    )
    request_table = request_table.reshape(st_count, capacity)
    asked = lax.all_to_all(request_table, "st", split_axis=0, concat_axis=0, tiled=True)
    both_weights = jnp.concatenate([key_weight, value_weight], axis=1)
    projected_store = project_rows(passage_store, passage_gain, both_weights)
    projected = jnp.take(projected_store, asked.reshape(-1), axis=0)
    returned = lax.all_to_all(
        projected.reshape(st_count, capacity * PLEN, 2 * head_width),
        "st",
        split_axis=0,
        concat_axis=0,
        tiled=True,
    )
    key_values = jnp.take(
        returned.reshape(st_count * capacity, PLEN, 2 * head_width), position_flat, axis=0
    )
    block_count = tok_rows // BLK
    key_values = key_values.reshape(block_count, NPB * PLEN, 2 * head_width)
    key_rows = key_values[:, :, :head_width].reshape(block_count, NPB * PLEN, local_heads, HD)
    values = key_values[:, :, head_width:].reshape(block_count, NPB * PLEN, local_heads, HD)
    query_blocks = queries.reshape(block_count, BLK, local_heads, HD)
    scores = jnp.einsum(
        "bqhd,bkhd->bhqk", query_blocks, key_rows, preferred_element_type=jnp.float32
    ) * HD ** (-0.5)
    row_max = jnp.max(scores, axis=-1, keepdims=True)
    weights = jnp.exp(scores - row_max)
    probabilities = (weights / jnp.sum(weights, axis=-1, keepdims=True)).astype(jnp.bfloat16)
    attended = jnp.einsum(
        "bhqk,bkhd->bqhd", probabilities, values, preferred_element_type=jnp.float32
    ).reshape(tok_rows, local_heads, HD)
    head_out = (attended * gating[:, :, None]).astype(jnp.bfloat16).reshape(tok_rows, head_width)
    crossed = jnp.dot(
        lax.all_gather(head_out, "tp", axis=1, tiled=True),
        out_weight,
        preferred_element_type=jnp.float32,
    )
    return (mixing + crossed).astype(jnp.bfloat16)


def solution(mesh):
    in_specs = (
        P(("grp", "st"), "tp"),
        P(),
        P("tp", None, None),
        P("tp"),
        P(None, "tp"),
        P(),
        P(None, "tp"),
        P(None, "tp"),
        P(None, "tp"),
        P(),
        P(("grp", "st"), None, None),
        P(("grp", "st"), None),
    )
    out_specs = P(("grp", "st"), "tp")
    return jax.shard_map(
        per_device, mesh=mesh, in_specs=in_specs, out_specs=out_specs, check_vma=False
    )
```

profile of v0, /device:TPU:0, one launch (start us, length us, event | category | flops | bytes accessed | tf_op | source)
XLA Modules:
  0.0 155.8 jit_solution(16865734827480352059)
XLA Ops:
  6.5 0.8 copy.41
  7.4 0.1 ne.86
  7.5 0.1 rem.47
  7.6 0.1 div.68
  7.7 0.2 convert_reduce_fusion
  7.9 0.1 select_reduce_fusion
  8.0 0.7 all_to_all.9
  8.6 6.3 %all-to-all-start = ((s32[4,1,8]{2,1,0:T(1,128)}), s32[4,1,8]{2,1,0:T(1,128)S(1)}, u32[]{:S(2)}, u32[]{:S(2)}) async-start(s32[4,1,8]{2,1,0:T(1,128)} %bitcast.9), calls=%async_computation | async-start | bytes 4096 | tf_op jit(solution)/shard_map/all_to_all | solution.py:97
  15.0 1.5 fusion.6
  16.5 6.5 %psum.7 = f32[1024]{0:T(1024)S(1)} all-reduce(f32[1024]{0:T(1024)S(1)} %fusion.6), channel_id=1, replica_groups=mesh['grp'=2,'st'=4,'tp'=4] {'tp'}, use_global_device_ids=true, to_apply=%region_1.0 | all-reduce | flops 1024 | bytes 8192 | tf_op jit(solution)/shard_map/psum | solution.py:51
  23.0 0.8 dynamic_slice.9
  23.8 2.5 %fusion.8 = bf16[1024,512]{1,0:T(8,128)(2,1)} fusion(bf16[1024,512]{1,0:T(8,128)(2,1)} %param.12, f32[512]{0:T(512)S(1)} %dynamic_slice.9, f32[1024]{0:T(1024)S(1)} %add_rsqrt_fusion.1), kind=kLoop, calls=%fused_computation.16 | loop fusion | flops 2097152 | bytes 2103296 | tf_op jit(solution)/shard_map/convert_element_type | solution.py:54
  26.4 4.1 %multiply_reduce_fusion = f32[24,64]{1,0:T(8,128)S(1)} fusion(bf16[24,64,2048]{2,1,0:T(8,128)(2,1)} %param.22), kind=kLoop, calls=%fused_computation.6 | loop fusion | flops 9435648 | bytes 6297600 | tf_op jit(solution)/shard_map/reduce_sum | solution.py:18
  30.5 4.6 %fusion.2 = bf16[1536,2048]{1,0:T(8,128)(2,1)S(1)} fusion(f32[2048]{0:T(1024)S(1)} %copy-done.4, f32[1536]{0:T(1024)S(1)} %rsqrt.16, bf16[24,64,2048]{2,1,0:T(8,128)(2,1)} %param.22), kind=kLoop, calls=%fused_computation.5 | loop fusion | flops 12582912 | bytes 12597248 | tf_op jit(solution)/shard_map/convert_element_type | solution.py:19
  35.1 4.8 %convolution_convert_fusion = bf16[1536,512]{1,0:T(8,128)(2,1)} fusion(bf16[1536,2048]{1,0:T(8,128)(2,1)S(1)} %fusion.2, bf16[2048,256]{1,0:T(8,128)(2,1)S(1)} %copy-done.6, bf16[2048,256]{1,0:T(8,128)(2,1)S(1)} %copy-done.7), kind=kOutput, calls=%fused_computation.7 | convolution fusion | flops 3226206208 | bytes 9961472 | tf_op jit(solution)/shard_map/dot_general | solution.py:25
  39.9 0.5 broadcast.275
  40.4 0.7 reduce.4
  41.1 0.1 reshape.267
  41.3 0.1 broadcast_in_dim.63
  41.4 2.1 %gather_fusion = bf16[32,64,512]{2,1,0:T(8,128)(2,1)S(1)} fusion(bf16[24,64,512]{2,1,0:T(8,128)(2,1)} %bitcast.73, s32[1024]{0:T(1024)S(1)} %pad_clamp_fusion.1), kind=kCustom, calls=%fused_computation | custom fusion | bytes 4194432 | tf_op jit(solution)/shard_map/jit(_take)/gather | solution.py:100
  43.5 1.6 %bitcast_select_fusion.1 = bf16[4,512,512]{2,1,0:T(8,128)(2,1)} fusion(pred[4,512]{1,0:T(4,128)(4,1)S(1)} %broadcast_in_dim.63, bf16[4,512,512]{2,1,0:T(8,128)(2,1)S(1)} %bitcast.66), kind=kLoop, calls=%fused_computation.21 | loop fusion | flops 1048576 | bytes 4196352 | tf_op jit(solution)/shard_map/jit(_take)/select_n | solution.py:100
  45.1 4.5 %all-to-all-start.1 = ((bf16[4,512,512]{2,1,0:T(8,128)(2,1)}), bf16[4,512,512]{2,1,0:T(8,128)(2,1)S(1)}, u32[]{:S(2)}, u32[]{:S(2)}) async-start(bf16[4,512,512]{2,1,0:T(8,128)(2,1)} %bitcast_select_fusion.1), calls=%async_computation.1 | async-start | bytes 4194304 | tf_op jit(solution)/shard_map/all_to_all | solution.py:101
  49.8 0.1 and.63
  49.9 0.1 broadcast_in_dim.58
  50.1 47.4 %all-to-all-done.1 = bf16[4,512,512]{2,1,0:T(8,128)(2,1)S(1)} async-done(((bf16[4,512,512]{2,1,0:T(8,128)(2,1)}), bf16[4,512,512]{2,1,0:T(8,128)(2,1)S(1)}, u32[]{:S(2)}, u32[]{:S(2)}) %all-to-all-start.1) | async-done | bytes 2097184 | tf_op jit(solution)/shard_map/all_to_all | solution.py:101
  97.4 2.0 %gather_fusion.1 = bf16[32,64,512]{2,1,0:T(8,128)(2,1)} fusion(bf16[32,64,512]{2,1,0:T(8,128)(2,1)S(1)} %bitcast.65, s32[1024]{0:T(1024)S(1)} %pad_clamp_fusion), kind=kCustom, calls=%fused_computation.1 | custom fusion | bytes 4194432 | tf_op jit(solution)/shard_map/jit(_take)/gather | solution.py:108
  99.4 1.8 %bitcast_select_fusion = bf16[8,256,512]{2,1,0:T(8,128)(2,1)S(1)} fusion(pred[8,256]{1,0:T(8,128)(4,1)S(1)} %broadcast_in_dim.58, bf16[8,256,512]{2,1,0:T(8,128)(2,1)} %bitcast.67), kind=kLoop, calls=%fused_computation.20 | loop fusion | flops 1048576 | bytes 4196352 | tf_op jit(solution)/shard_map/jit(_take)/select_n | solution.py:108
  101.2 1.2 fusion.46
  102.4 1.5 copy.46
  103.9 1.3 copy.45
  105.2 3.7 %convolution_convert_fusion.1 = bf16[1024,256]{1,0:T(8,128)(2,1)S(1)} fusion(bf16[1024,2048]{1,0:T(8,128)(2,1)} %all-gather.3.cloned.1.call-done, bf16[2048,256]{1,0:T(8,128)(2,1)} %param.16), kind=kOutput, calls=%fused_computation.31 | convolution fusion | flops 1074003968 | bytes 5767168 | tf_op jit(solution)/shard_map/dot_general | solution.py:78
  108.9 0.1 reshape.270
  109.1 1.0 fusion.47
  110.1 1.8 %fusion.22 = f32[8,2,128,256]{3,2,1,0:T(8,128)} fusion(bf16[8,256,2,128]{1,3,2,0:T(8,128)(2,1)S(1)} %bitcast.70, bf16[8,128,2,128]{3,2,1,0:T(2,128)(2,1)S(1)} %reshape.270), kind=kOutput, calls=%fused_computation.41 | convolution fusion | flops 134217728 | bytes 3670016 | tf_op jit(solution)/shard_map/bqhd,bkhd->bhqk/dot_general | solution.py:116
  111.8 5.7 %convolution_bitcast_fusion = f32[8,128,2,128]{1,3,2,0:T(8,128)S(1)} fusion(bf16[8,256,2,128]{1,3,2,0:T(8,128)(2,1)} %bitcast.74, f32[8,2,128]{2,1,0:T(2,128)S(1)} %fusion.47, f32[8,2,128,256]{3,2,1,0:T(8,128)} %fusion.22), kind=kOutput, calls=%fused_computation.30 | convolution fusion | flops 136317184 | bytes 4202496 | tf_op jit(solution)/shard_map/bhqk,bkhd->bqhd/dot_general | solution.py:122
  117.5 0.6 copy.49
  118.1 3.4 %fusion.18 = f32[1024,2]{0,1:T(2,128)S(1)} fusion(bf16[1024,2048]{1,0:T(8,128)(2,1)} %all-gather.3.cloned.1.call-done, bf16[2048,8]{0,1:T(8,128)(2,1)} %param.17, s32[]{:T(128)S(6)} %select_n.108), kind=kOutput, calls=%fused_computation.35 | convolution fusion | flops 8394752 | bytes 4210692 | tf_op jit(solution)/shard_map/dot_general | solution.py:79
  121.5 1.0 fusion.19
  122.5 0.4 copy-done.1
  122.9 0.3 convert.2
  123.2 1.6 %fusion.12 = f32[4,512,2,128]{1,2,3,0:T(2,128)S(1)} fusion(f32[4,512,2,128]{1,3,2,0:T(8,128)S(1)} %bitcast.68), kind=kOutput, calls=%fused_computation.22 | output fusion | flops 66584576 | bytes 4194304 | tf_op jit(solution)/shard_map/reduce-window
  124.9 1.3 copy-done.2
  126.2 2.4 %broadcast_add_fusion = f32[4,512,2,128]{1,2,3,0:T(2,128)S(1)} fusion(f32[4,512,2,128]{1,2,3,0:T(2,128)} %copy-done.2, f32[4,512,2]{1,2,0:T(2,128)S(1)} %slice.21), kind=kLoop, calls=%fused_computation.39 | loop fusion | flops 524288 | bytes 4210688 | tf_op jit(solution)/shard_map/reduce_window_sum
  128.6 1.7 %copy.40 = f32[4,512,2,128]{1,3,2,0:T(8,128)} copy(f32[4,512,2,128]{1,2,3,0:T(2,128)S(1)} %broadcast_add_fusion) | data formatting | bytes 4194304 | tf_op jit(solution)/shard_map/reduce_window_sum
  130.3 3.1 %fusion.14 = bf16[4,256,512]{2,1,0:T(8,128)(2,1)S(1)} fusion(f32[4,256,512]{2,1,0:T(8,128)} %bitcast.64, s32[]{:T(128)S(6)} %select_n.96, f32[256]{0:T(256)S(1)} %minimum_convert_fusion, bf16[4,256,512]{2,1,0:T(8,128)(2,1)S(1)} %bitcast.63), kind=kLoop, calls=%fused_computation.27 | loop fusion | flops 2621440 | bytes 4195332 | tf_op jit(solution)/shard_map/convert_element_type | solution.py:68
  133.4 10.9 %all-gather.5.cloned.1.call-done = bf16[1024,1024]{0,1:T(8,128)(2,1)} async-done(((bf16[1024,256]{0,1:T(8,128)(2,1)}), bf16[1024,1024]{0,1:T(8,128)(2,1)}) %all-gather.5.cloned.1.call-update) | async-done | bytes 2097168 | tf_op jit(solution)/shard_map/all_gather | solution.py:127
  144.3 2.9 %fusion.50 = f32[1024,512]{1,0:T(8,128)S(1)} fusion(bf16[1024,1024]{0,1:T(8,128)(2,1)} %all-gather.5.cloned.1.call-done, bf16[1024,512]{1,0:T(8,128)(2,1)S(1)} %copy-done), kind=kOutput, calls=%fused_computation.83 | convolution fusion | flops 1073741824 | bytes 5242880 | tf_op jit(solution)/shard_map/dot_general | solution.py:126
  147.2 1.7 %add_convert_fusion = bf16[1024,512]{1,0:T(8,128)(2,1)} fusion(f32[1024,512]{1,0:T(8,128)S(1)} %fusion.50, bf16[1024,512]{1,0:T(8,128)(2,1)S(1)} %bitcast.71, f32[512]{0:T(512)S(1)} %copy-done.5, bf16[1,512,512]{2,1,0:T(8,128)(2,1)S(1)} %copy-done.3), kind=kOutput, calls=%fused_computation.24 | convolution fusion | flops 538443776 | bytes 4720640 | tf_op jit(solution)/shard_map/dot_general | solution.py:72
  (41 shorter events, 0.6 us)
Async XLA Ops:
  6.5 137.8 %copy-start = (bf16[1024,512]{1,0:T(8,128)(2,1)S(1)}, bf16[1024,512]{1,0:T(8,128)(2,1)}, u32[]{:S(2)}) copy-start(bf16[1024,512]{1,0:T(8,128)(2,1)} %param.20) | copy-start | bytes 3145732
  8.6 31.3 %all-to-all-start = ((s32[4,1,8]{2,1,0:T(1,128)}), s32[4,1,8]{2,1,0:T(1,128)S(1)}, u32[]{:S(2)}, u32[]{:S(2)}) async-start(s32[4,1,8]{2,1,0:T(1,128)} %bitcast.9), calls=%async_computation | async-start | bytes 4096 | tf_op jit(solution)/shard_map/all_to_all | solution.py:97
  15.0 90.2 %all-gather.3.cloned.1.call-start = ((), (), s32[]{:S(2)}) async-start(), calls=%async_computation.2 | async-start | bytes 5242880 | tf_op jit(solution)/shard_map/all_gather | solution.py:77
  26.3 4.2 %copy-start.4 = (f32[2048]{0:T(1024)S(1)}, f32[2048]{0:T(1024)}, u32[]{:S(2)}) copy-start(f32[2048]{0:T(1024)} %param.21) | copy-start | bytes 24580
  30.5 4.6 %copy-start.6 = (bf16[2048,256]{1,0:T(8,128)(2,1)S(1)}, bf16[2048,256]{1,0:T(8,128)(2,1)}, u32[]{:S(2)}) copy-start(bf16[2048,256]{1,0:T(8,128)(2,1)} %param.19) | copy-start | bytes 3145732
  30.5 4.6 %copy-start.7 = (bf16[2048,256]{1,0:T(8,128)(2,1)S(1)}, bf16[2048,256]{1,0:T(8,128)(2,1)}, u32[]{:S(2)}) copy-start(bf16[2048,256]{1,0:T(8,128)(2,1)} %param.18) | copy-start | bytes 3145732
  45.1 52.4 %all-to-all-start.1 = ((bf16[4,512,512]{2,1,0:T(8,128)(2,1)}), bf16[4,512,512]{2,1,0:T(8,128)(2,1)S(1)}, u32[]{:S(2)}, u32[]{:S(2)}) async-start(bf16[4,512,512]{2,1,0:T(8,128)(2,1)} %bitcast_select_fusion.1), calls=%async_computation.1 | async-start | bytes 4194304 | tf_op jit(solution)/shard_map/all_to_all | solution.py:101
  49.6 94.7 %all-gather.5.cloned.1.call-start = ((), (), s32[]{:S(2)}) async-start(), calls=%async_computation.3 | async-start | bytes 2621440 | tf_op jit(solution)/shard_map/all_gather | solution.py:127
  121.5 1.4 copy-start.1
  124.9 1.3 copy-start.2
  133.4 13.9 %copy-start.3 = (bf16[1,512,512]{2,1,0:T(8,128)(2,1)S(1)}, bf16[1,512,512]{2,1,0:T(8,128)(2,1)}, u32[]{:S(2)}) copy-start(bf16[1,512,512]{2,1,0:T(8,128)(2,1)} %param.14) | copy-start | bytes 1572868
  133.4 13.9 %copy-start.5 = (f32[512]{0:T(512)S(1)}, f32[512]{0:T(512)}, u32[]{:S(2)}) copy-start(f32[512]{0:T(512)} %param.15) | copy-start | bytes 6148
Sparse Core Ops, SparseCore 0:
  26.5 35.3 all-gather.2
  122.6 21.6 all-gather.4
where the time goes:
time: 156 us
  waiting for transfers between devices  58.3 us (37%)
  other arithmetic  25.5 us (16%)
  matrix products  24.9 us (16%)
  local copies, waits for them, and re-layouts  16 us (10%)
  between operations  13.6 us (9%)
  starting transfers between devices  10.9 us (7%)
  blocking collectives  6.52 us (4%)
    all_to_all x1, waiting for transfers between devices, per_device(): lax.all_to_all(projected.reshape(st_count, capacity * PLEN, 2 * head_widt...  47.4 us
    all_gather x1, waiting for transfers between devices, per_device(): lax.all_gather(head_out, 'tp', axis=1, tiled=True)  10.9 us
    psum x1, blocking collectives, per_device(): square_sums = lax.psum(jnp.sum(wide_tokens * wide_tokens, axis=1), 'tp')  6.52 us
    all_to_all x1, starting transfers between devices, per_device(): lax.all_to_all(request_table, 'st', split_axis=0, concat_axis=0, tiled=True)  6.35 us
    dot_general x1, matrix products, per_device(): jnp.einsum('bhqk,bkhd->bqhd', probabilities, values, preferred_element_ty...  5.65 us
    dot_general x1, matrix products, project_rows(): jnp.dot(flat_rows, both_weights, preferred_element_type=jnp.float32)  4.79 us
    convert_element_type x1, other arithmetic, normalize_rows(): return (wide_rows * inverse * passage_gain).astype(jnp.bfloat16)  4.56 us
    all_to_all x1, starting transfers between devices, per_device(): lax.all_to_all(projected.reshape(st_count, capacity * PLEN, 2 * head_widt...  4.53 us
  transfers between devices with their start and end apart: 4, of which 2 were waited for; matrix products, arithmetic and copies ran while one was open for 26% of the time, Pallas kernels for 0%

commit v1 on v0

--- a/solution.py
+++ b/solution.py
@@ -11,6 +11,10 @@
 PLEN = 64
 P_DEV = 24
 epsilon = 1e-06
+
+
+def supply_all_files(original):
+    return jnp.concatenate(lax.all_gather(original, "tp"), axis=1)
 
 
 def normalize_rows(fetched, passage_gain):
@@ -123,11 +127,7 @@
         "bhqk,bkhd->bqhd", probabilities, values, preferred_element_type=jnp.float32
     ).reshape(tok_rows, local_heads, HD)
     head_out = (attended * gating[:, :, None]).astype(jnp.bfloat16).reshape(tok_rows, head_width)
-    crossed = jnp.dot(
-        lax.all_gather(head_out, "tp", axis=1, tiled=True),
-        out_weight,
-        preferred_element_type=jnp.float32,
-    )
+    crossed = jnp.dot(supply_all_files(head_out), out_weight, preferred_element_type=jnp.float32)
     return (mixing + crossed).astype(jnp.bfloat16)
 
 

time: 156 us -> 163 us (1.045)
  local copies, waits for them, and re-layouts: 16 us -> 21.8 us
    all_gather x0 -> x1, local copies, waits for them, and re-layouts: none -> 3.96 us  [supply_all_files(): return jnp.concatenate(lax.all_gather(original, 'tp'), axis=1)]
    convert_element_type x0 -> x1, local copies, waits for them, and re-layouts: none -> 2.04 us  [per_device(): (attended * gating[:, :, None]).astype(jnp.bfloat16)]
  transfers between devices with their start and end apart: 4 -> 4, of which waited for: 2 -> 2; matrix products, arithmetic and copies ran while one was open for 26% -> 25% of each run, Pallas kernels for 0% -> 0%
where the time goes in v1:
time: 163 us; the launch traced here: 162 us
  waiting for transfers between devices  58.8 us (36%)
  other arithmetic  25.3 us (16%)
  matrix products  25 us (15%)
  local copies, waits for them, and re-layouts  21.8 us (13%)
  between operations  13.6 us (8%)
  starting transfers between devices  10.9 us (7%)
  blocking collectives  6.52 us (4%)
    all_to_all x1, waiting for transfers between devices, per_device(): lax.all_to_all(projected.reshape(st_count, capacity * PLEN, 2 * head_widt...  47.4 us
    all_gather x1, waiting for transfers between devices, supply_all_files(): return jnp.concatenate(lax.all_gather(original, 'tp'), axis=1)  11.4 us
    psum x1, blocking collectives, per_device(): square_sums = lax.psum(jnp.sum(wide_tokens * wide_tokens, axis=1), 'tp')  6.52 us
    all_to_all x1, starting transfers between devices, per_device(): lax.all_to_all(request_table, 'st', split_axis=0, concat_axis=0, tiled=True)  6.35 us
    dot_general x1, matrix products, per_device(): jnp.einsum('bhqk,bkhd->bqhd', probabilities, values, preferred_element_ty...  5.65 us
    dot_general x1, matrix products, project_rows(): jnp.dot(flat_rows, both_weights, preferred_element_type=jnp.float32)  4.79 us
    convert_element_type x1, other arithmetic, normalize_rows(): return (wide_rows * inverse * passage_gain).astype(jnp.bfloat16)  4.56 us
    all_to_all x1, starting transfers between devices, per_device(): lax.all_to_all(projected.reshape(st_count, capacity * PLEN, 2 * head_widt...  4.53 us
  transfers between devices with their start and end apart: 4, of which 2 were waited for; matrix products, arithmetic and copies ran while one was open for 25% of the time, Pallas kernels for 0%

profile of v1, /device:TPU:0, one launch (start us, length us, event | category | flops | bytes accessed | tf_op | source)
XLA Modules:
  0.0 161.9 jit_solution(18299036360403414874)
XLA Ops:
  6.5 0.8 copy.43
  7.4 0.1 ne.86
  7.7 0.2 convert_reduce_fusion
  7.9 0.1 select_reduce_fusion
  8.0 0.7 all_to_all.9
  8.6 6.3 %all-to-all-start = ((s32[4,1,8]{2,1,0:T(1,128)}), s32[4,1,8]{2,1,0:T(1,128)S(1)}, u32[]{:S(2)}, u32[]{:S(2)}) async-start(s32[4,1,8]{2,1,0:T(1,128)} %bitcast.9), calls=%async_computation | async-start | bytes 4096 | tf_op jit(solution)/shard_map/all_to_all | solution.py:101
  15.0 1.5 fusion.6
  16.5 6.5 %psum.7 = f32[1024]{0:T(1024)S(1)} all-reduce(f32[1024]{0:T(1024)S(1)} %fusion.6), channel_id=1, replica_groups=mesh['grp'=2,'st'=4,'tp'=4] {'tp'}, use_global_device_ids=true, to_apply=%region_1.0 | all-reduce | flops 1024 | bytes 8192 | tf_op jit(solution)/shard_map/psum | solution.py:55
  23.0 0.8 dynamic_slice.9
  23.8 2.5 %fusion.8 = bf16[1024,512]{1,0:T(8,128)(2,1)} fusion(bf16[1024,512]{1,0:T(8,128)(2,1)} %param.12, f32[512]{0:T(512)S(1)} %dynamic_slice.9, f32[1024]{0:T(1024)S(1)} %add_rsqrt_fusion.1), kind=kLoop, calls=%fused_computation.16 | loop fusion | flops 2097152 | bytes 2103296 | tf_op jit(solution)/shard_map/convert_element_type | solution.py:58
  26.4 4.1 %multiply_reduce_fusion = f32[24,64]{1,0:T(8,128)S(1)} fusion(bf16[24,64,2048]{2,1,0:T(8,128)(2,1)} %param.22), kind=kLoop, calls=%fused_computation.6 | loop fusion | flops 9435648 | bytes 6297600 | tf_op jit(solution)/shard_map/reduce_sum | solution.py:22
  30.5 4.6 %fusion.2 = bf16[1536,2048]{1,0:T(8,128)(2,1)S(1)} fusion(f32[2048]{0:T(1024)S(1)} %copy-done.4, f32[1536]{0:T(1024)S(1)} %rsqrt.16, bf16[24,64,2048]{2,1,0:T(8,128)(2,1)} %param.22), kind=kLoop, calls=%fused_computation.5 | loop fusion | flops 12582912 | bytes 12597248 | tf_op jit(solution)/shard_map/convert_element_type | solution.py:23
  35.1 4.8 %convolution_convert_fusion = bf16[1536,512]{1,0:T(8,128)(2,1)} fusion(bf16[1536,2048]{1,0:T(8,128)(2,1)S(1)} %fusion.2, bf16[2048,256]{1,0:T(8,128)(2,1)S(1)} %copy-done.6, bf16[2048,256]{1,0:T(8,128)(2,1)S(1)} %copy-done.7), kind=kOutput, calls=%fused_computation.7 | convolution fusion | flops 3226206208 | bytes 9961472 | tf_op jit(solution)/shard_map/dot_general | solution.py:29
  39.9 0.5 broadcast.276
  40.4 0.7 reduce.4
  41.1 0.1 reshape.292
  41.3 0.1 broadcast_in_dim.63
  41.4 2.1 %gather_fusion = bf16[32,64,512]{2,1,0:T(8,128)(2,1)S(1)} fusion(bf16[24,64,512]{2,1,0:T(8,128)(2,1)} %bitcast.73, s32[1024]{0:T(1024)S(1)} %pad_clamp_fusion.1), kind=kCustom, calls=%fused_computation | custom fusion | bytes 4194432 | tf_op jit(solution)/shard_map/jit(_take)/gather | solution.py:104
  43.5 1.6 bitcast_select_fusion.1
  45.1 4.5 %all-to-all-start.1 = ((bf16[4,512,512]{2,1,0:T(8,128)(2,1)}), bf16[4,512,512]{2,1,0:T(8,128)(2,1)S(1)}, u32[]{:S(2)}, u32[]{:S(2)}) async-start(bf16[4,512,512]{2,1,0:T(8,128)(2,1)} %bitcast_select_fusion.1), calls=%async_computation.1 | async-start | bytes 4194304 | tf_op jit(solution)/shard_map/all_to_all | solution.py:105
  49.8 0.1 and.63
  49.9 0.1 broadcast_in_dim.58
  50.1 47.4 %all-to-all-done.1 = bf16[4,512,512]{2,1,0:T(8,128)(2,1)S(1)} async-done(((bf16[4,512,512]{2,1,0:T(8,128)(2,1)}), bf16[4,512,512]{2,1,0:T(8,128)(2,1)S(1)}, u32[]{:S(2)}, u32[]{:S(2)}) %all-to-all-start.1) | async-done | bytes 2097184 | tf_op jit(solution)/shard_map/all_to_all | solution.py:105
  97.4 2.0 %gather_fusion.1 = bf16[32,64,512]{2,1,0:T(8,128)(2,1)} fusion(bf16[32,64,512]{2,1,0:T(8,128)(2,1)S(1)} %bitcast.66, s32[1024]{0:T(1024)S(1)} %pad_clamp_fusion), kind=kCustom, calls=%fused_computation.1 | custom fusion | bytes 4194432 | tf_op jit(solution)/shard_map/jit(_take)/gather | solution.py:112
  99.4 1.8 %bitcast_select_fusion = bf16[8,256,512]{2,1,0:T(8,128)(2,1)S(1)} fusion(pred[8,256]{1,0:T(8,128)(4,1)S(1)} %broadcast_in_dim.58, bf16[8,256,512]{2,1,0:T(8,128)(2,1)} %bitcast.68), kind=kLoop, calls=%fused_computation.20 | loop fusion | flops 1048576 | bytes 4196352 | tf_op jit(solution)/shard_map/jit(_take)/select_n | solution.py:112
  101.2 1.2 fusion.46
  102.4 1.5 copy.48
  103.9 1.3 copy.47
  105.2 3.7 %convolution_convert_fusion.1 = bf16[1024,256]{1,0:T(8,128)(2,1)S(1)} fusion(bf16[1024,2048]{1,0:T(8,128)(2,1)} %all-gather.3.cloned.1.call-done, bf16[2048,256]{1,0:T(8,128)(2,1)} %param.16), kind=kOutput, calls=%fused_computation.31 | convolution fusion | flops 1074003968 | bytes 5767168 | tf_op jit(solution)/shard_map/dot_general | solution.py:82
  108.9 0.1 reshape.295
  109.1 1.0 fusion.47
  110.1 1.8 %fusion.22 = f32[8,2,128,256]{3,2,1,0:T(8,128)} fusion(bf16[8,256,2,128]{1,3,2,0:T(8,128)(2,1)S(1)} %bitcast.71, bf16[8,128,2,128]{3,2,1,0:T(2,128)(2,1)S(1)} %reshape.295), kind=kOutput, calls=%fused_computation.41 | convolution fusion | flops 134217728 | bytes 3670016 | tf_op jit(solution)/shard_map/bqhd,bkhd->bhqk/dot_general | solution.py:120
  111.8 5.7 %convolution_bitcast_fusion = f32[8,128,2,128]{1,3,2,0:T(8,128)S(1)} fusion(bf16[8,256,2,128]{1,3,2,0:T(8,128)(2,1)} %bitcast.75, f32[8,2,128]{2,1,0:T(2,128)S(1)} %fusion.47, f32[8,2,128,256]{3,2,1,0:T(8,128)} %fusion.22), kind=kOutput, calls=%fused_computation.30 | convolution fusion | flops 136317184 | bytes 4202496 | tf_op jit(solution)/shard_map/bhqk,bkhd->bqhd/dot_general | solution.py:126
  117.5 0.6 copy.51
  118.1 0.2 reshape.297
  118.3 3.4 %fusion.18 = f32[1024,2]{0,1:T(2,128)S(1)} fusion(bf16[1024,2048]{1,0:T(8,128)(2,1)} %all-gather.3.cloned.1.call-done, bf16[2048,8]{0,1:T(8,128)(2,1)} %param.17, s32[]{:T(128)S(6)} %select_n.108), kind=kOutput, calls=%fused_computation.35 | convolution fusion | flops 8394752 | bytes 4210692 | tf_op jit(solution)/shard_map/dot_general | solution.py:83
  121.7 0.9 fusion.19
  122.6 2.0 %copy.52 = bf16[1,1024,256]{2,1,0:T(8,128)(2,1)} copy(bf16[1,1024,256]{1,2,0:T(8,128)(2,1)} %fusion.19) | data formatting | bytes 1048576 | tf_op jit(solution)/shard_map/convert_element_type | solution.py:129
  124.7 0.3 convert.2
  124.9 1.6 %fusion.12 = f32[4,512,2,128]{1,2,3,0:T(2,128)S(1)} fusion(f32[4,512,2,128]{1,3,2,0:T(8,128)S(1)} %bitcast.69), kind=kOutput, calls=%fused_computation.22 | output fusion | flops 66584576 | bytes 4194304 | tf_op jit(solution)/shard_map/reduce-window
  126.6 1.3 copy-done.2
  128.0 2.3 %broadcast_add_fusion = f32[4,512,2,128]{1,2,3,0:T(2,128)S(1)} fusion(f32[4,512,2,128]{1,2,3,0:T(2,128)} %copy-done.2, f32[4,512,2]{1,2,0:T(2,128)S(1)} %slice.21), kind=kLoop, calls=%fused_computation.39 | loop fusion | flops 524288 | bytes 4210688 | tf_op jit(solution)/shard_map/reduce_window_sum
  130.3 1.7 %copy.42 = f32[4,512,2,128]{1,3,2,0:T(8,128)} copy(f32[4,512,2,128]{1,2,3,0:T(2,128)S(1)} %broadcast_add_fusion) | data formatting | bytes 4194304 | tf_op jit(solution)/shard_map/reduce_window_sum
  132.0 3.1 %fusion.14 = bf16[4,256,512]{2,1,0:T(8,128)(2,1)S(1)} fusion(f32[4,256,512]{2,1,0:T(8,128)} %bitcast.65, s32[]{:T(128)S(6)} %select_n.96, f32[256]{0:T(256)S(1)} %minimum_convert_fusion, bf16[4,256,512]{2,1,0:T(8,128)(2,1)S(1)} %bitcast.64), kind=kLoop, calls=%fused_computation.27 | loop fusion | flops 2621440 | bytes 4195332 | tf_op jit(solution)/shard_map/convert_element_type | solution.py:72
  135.0 11.4 %all-gather.5.cloned.1.call-done = bf16[4,1024,256]{2,1,0:T(8,128)(2,1)} async-done(((bf16[1,1024,256]{2,1,0:T(8,128)(2,1)}), bf16[4,1024,256]{2,1,0:T(8,128)(2,1)}) %all-gather.5.cloned.1.call-update) | async-done | bytes 2097168 | tf_op jit(solution)/shard_map/all_gather | solution.py:17
  146.5 4.0 %copy.53 = bf16[4,1024,256]{1,2,0:T(8,128)(2,1)} copy(bf16[4,1024,256]{2,1,0:T(8,128)(2,1)} %all-gather.5.cloned.1.call-done) | data formatting | bytes 4194304 | tf_op jit(solution)/shard_map/all_gather | solution.py:17
  150.4 2.9 %fusion.50 = f32[1024,512]{1,0:T(8,128)S(1)} fusion(bf16[1024,1024]{0,1:T(8,128)(2,1)} %bitcast.74, bf16[1024,512]{1,0:T(8,128)(2,1)S(1)} %copy-done), kind=kOutput, calls=%fused_computation.83 | convolution fusion | flops 1073741824 | bytes 5242880 | tf_op jit(solution)/shard_map/dot_general | solution.py:130
  153.4 1.7 %add_convert_fusion = bf16[1024,512]{1,0:T(8,128)(2,1)} fusion(f32[1024,512]{1,0:T(8,128)S(1)} %fusion.50, bf16[1024,512]{1,0:T(8,128)(2,1)S(1)} %bitcast.72, f32[512]{0:T(512)S(1)} %copy-done.5, bf16[1,512,512]{2,1,0:T(8,128)(2,1)S(1)} %copy-done.3), kind=kOutput, calls=%fused_computation.24 | convolution fusion | flops 538443776 | bytes 4720640 | tf_op jit(solution)/shard_map/dot_general | solution.py:76
  (44 shorter events, 0.8 us)
Async XLA Ops:
  6.5 143.9 %copy-start = (bf16[1024,512]{1,0:T(8,128)(2,1)S(1)}, bf16[1024,512]{1,0:T(8,128)(2,1)}, u32[]{:S(2)}) copy-start(bf16[1024,512]{1,0:T(8,128)(2,1)} %param.20) | copy-start | bytes 3145732
  8.6 31.3 %all-to-all-start = ((s32[4,1,8]{2,1,0:T(1,128)}), s32[4,1,8]{2,1,0:T(1,128)S(1)}, u32[]{:S(2)}, u32[]{:S(2)}) async-start(s32[4,1,8]{2,1,0:T(1,128)} %bitcast.9), calls=%async_computation | async-start | bytes 4096 | tf_op jit(solution)/shard_map/all_to_all | solution.py:101
  15.0 90.2 %all-gather.3.cloned.1.call-start = ((), (), s32[]{:S(2)}) async-start(), calls=%async_computation.2 | async-start | bytes 5242880 | tf_op jit(solution)/shard_map/all_gather | solution.py:81
  26.3 4.2 %copy-start.4 = (f32[2048]{0:T(1024)S(1)}, f32[2048]{0:T(1024)}, u32[]{:S(2)}) copy-start(f32[2048]{0:T(1024)} %param.21) | copy-start | bytes 24580
  30.5 4.6 %copy-start.6 = (bf16[2048,256]{1,0:T(8,128)(2,1)S(1)}, bf16[2048,256]{1,0:T(8,128)(2,1)}, u32[]{:S(2)}) copy-start(bf16[2048,256]{1,0:T(8,128)(2,1)} %param.19) | copy-start | bytes 3145732
  30.5 4.6 %copy-start.7 = (bf16[2048,256]{1,0:T(8,128)(2,1)S(1)}, bf16[2048,256]{1,0:T(8,128)(2,1)}, u32[]{:S(2)}) copy-start(bf16[2048,256]{1,0:T(8,128)(2,1)} %param.18) | copy-start | bytes 3145732
  45.1 52.4 %all-to-all-start.1 = ((bf16[4,512,512]{2,1,0:T(8,128)(2,1)}), bf16[4,512,512]{2,1,0:T(8,128)(2,1)S(1)}, u32[]{:S(2)}, u32[]{:S(2)}) async-start(bf16[4,512,512]{2,1,0:T(8,128)(2,1)} %bitcast_select_fusion.1), calls=%async_computation.1 | async-start | bytes 4194304 | tf_op jit(solution)/shard_map/all_to_all | solution.py:105
  49.6 96.9 %all-gather.5.cloned.1.call-start = ((), (), s32[]{:S(2)}) async-start(), calls=%async_computation.3 | async-start | bytes 2621440 | tf_op jit(solution)/shard_map/all_gather | solution.py:17
  121.7 3.0 %copy-start.1 = (bf16[1024,512]{1,0:T(8,128)(2,1)S(1)}, bf16[1024,512]{1,0:T(8,128)(2,1)}, u32[]{:S(2)}) copy-start(bf16[1024,512]{1,0:T(8,128)(2,1)} %fusion.8) | copy-start | bytes 3145732
  126.6 1.3 copy-start.2
  150.4 2.9 %copy-start.3 = (bf16[1,512,512]{2,1,0:T(8,128)(2,1)S(1)}, bf16[1,512,512]{2,1,0:T(8,128)(2,1)}, u32[]{:S(2)}) copy-start(bf16[1,512,512]{2,1,0:T(8,128)(2,1)} %param.14) | copy-start | bytes 1572868
  150.4 3.0 %copy-start.5 = (f32[512]{0:T(512)S(1)}, f32[512]{0:T(512)}, u32[]{:S(2)}) copy-start(f32[512]{0:T(512)} %param.15) | copy-start | bytes 6148
Sparse Core Ops, SparseCore 0:
  26.5 35.3 all-gather.2
  124.8 21.6 all-gather.4
